TPU v7x, 512 devices: a 4x2x32 block of a 4x8x32 slice. The times are simulated.
512 devices in a mesh: grp: 2 (over y), ep: 64 (over z, core), tp: 4 (over x).
Axes of the slice: x: 4, y: 2, z: 32, core: 2. Of those that a mesh axis runs over, the one named last changes fastest.
The devices are a block of a 4x8x32 slice.
Arguments:
- tokens: bfloat16 [24576, 2048], P(('grp', 'ep')), parts along dimension 0, may hold values from -6 to 6
- norm_gain: float32 [2048], replicated, may hold values from 0.1 to 1.9
- w_gate: bfloat16 [64, 2048, 1024], P('ep', None, 'tp'), may hold values from -0.3125 to 0.3125
- w_up: bfloat16 [64, 2048, 1024], P('ep', None, 'tp'), may hold values from -0.3125 to 0.3125
- w_down: bfloat16 [64, 1024, 2048], P('ep', 'tp'), may hold values from -0.09375 to 0.09375
- expert_ids: int32 [24576, 4], P(('grp', 'ep')), parts along dimension 0, may hold values from 0 to 63, all different within a row; in each aligned block of 192 rows (0 to 191, 192 to 383, ...) at most 16 rows name the same one
- gate_weights: float32 [24576, 4], P(('grp', 'ep')), parts along dimension 0, may hold values from 0.1 to 1
Outputs:
- mixed: bfloat16 [24576, 2048], P(('grp', 'ep'), 'tp'), parts along dimension 0
There are 2 independent parts, one for each index of `grp`. A program takes and returns all parts, laid end to end along the dimension named above; an argument that names none is the same for every part. Nothing has to cross between parts.
Inputs may be any that keep to these rules, and one draw needn't show every extreme that they name: `expert_ids`: each row names 4 different experts; among the rows of one index of ep, no expert is named by more than 16 rows, a bound that some block reaches.
All inputs are finite; a program needn't handle non-finite values.
Results may differ from a plain program's by a relative error of at most 0.012.
Values may be sent and summed in bfloat16 or wider, within the bound.
A program may use at most 64 MiB of HBM per device.

v0:
```python
import jax
import jax.numpy as jnp
from jax import lax
from jax.sharding import Mesh
from jax.sharding import PartitionSpec as P

EP = ("ep_0", "ep_1")
GRP_EP = ("grp", "ep_0", "ep_1")
epsilon = 1e-06
clamp_limit = 7.0
swish_alpha = 1.702


def cut_along(value, dim, devices):
    before, after = (value.shape[:dim], value.shape[dim + 1 :])
    return jnp.moveaxis(value.reshape(*before, devices, -1, *after), dim, 0)


def laid_out(blocks, dim):
    blocks = jnp.moveaxis(blocks, 0, dim)
    shape = blocks.shape
    return blocks.reshape(*shape[:dim], shape[dim] * shape[dim + 1], *shape[dim + 2 :])


def turned_blocks(blocks, axes, turns):
    inside = blocks.shape[1:]
    whole = blocks.reshape(*(lax.axis_size(a) for a in axes), *inside)
    for k in turns:
        whole = lax.all_to_all(whole, axes[k], k, k, tiled=True)
    return whole.reshape(-1, *inside)


def exchange_by_chip(value, groups, turns, split_dim, concat_dim):
    devices = lax.axis_size(groups[0]) * lax.axis_size(groups[1])
    blocks = cut_along(value, split_dim, devices)
    return laid_out(turned_blocks(blocks, groups, turns), concat_dim)


def sent_and_summed(value, axis, dim):
    blocks = cut_along(value, dim, lax.axis_size(axis))
    arrived = lax.all_to_all(blocks, axis, split_axis=0, concat_axis=0, tiled=True)
    return arrived.astype(jnp.float32).sum(axis=0)


def rms_norm(tokens, norm_gain):
    widened = tokens.astype(jnp.float32)
    scaled = widened * lax.rsqrt(jnp.mean(widened * widened, axis=-1, keepdims=True) + epsilon)
    return (scaled * norm_gain).astype(jnp.bfloat16)


def body(tokens, norm_gain, w_gate, w_up, w_down, expert_ids, gate_weights):
    tok_rows, model_width = tokens.shape
    top_count = expert_ids.shape[1]
    ep_count = lax.axis_size(EP)
    tp_count = lax.axis_size("tp")
    local_experts = w_gate.shape[0]
    experts_all = local_experts * ep_count
    capacity = min(tok_rows, tok_rows * top_count * 4 // (3 * experts_all))
    normed = rms_norm(tokens, norm_gain)
    flat_ids = expert_ids.reshape(-1)
    onehot = (flat_ids[:, None] == jnp.arange(experts_all, dtype=jnp.int32)[None, :]).astype(
        jnp.int32
    )
    before = jnp.cumsum(onehot, axis=0) - onehot
    slot_index = jnp.sum(before * onehot, axis=1)
    dest_row = flat_ids * capacity + slot_index
    owner_tok = jnp.arange(tok_rows * top_count, dtype=jnp.int32) // top_count
    slot_table = (
        jnp.full((experts_all * capacity,), tok_rows, jnp.int32).at[dest_row].set(owner_tok)
    )
    padded = jnp.concatenate([normed, jnp.zeros((1, model_width), jnp.bfloat16)], axis=0)
    send_buffer = padded[slot_table].reshape(experts_all, capacity, model_width)
    col_share = model_width // tp_count
    col_part = lax.dynamic_slice_in_dim(send_buffer, lax.axis_index("tp") * col_share, col_share, 2)
    received = exchange_by_chip(col_part, ("ep_0", "ep_1"), (1, 0), 0, 0)
    received = lax.all_gather(received, "tp", axis=2, tiled=True)
    expert_rows = received.reshape(ep_count, local_experts, capacity, model_width)
    gate_pre = jnp.einsum("sjcd,jdf->sjcf", expert_rows, w_gate, preferred_element_type=jnp.float32)
    up_pre = jnp.einsum("sjcd,jdf->sjcf", expert_rows, w_up, preferred_element_type=jnp.float32)
    gated = jnp.minimum(gate_pre, clamp_limit)
    linear = jnp.clip(up_pre, -clamp_limit, clamp_limit)
    activated = (gated * jax.nn.sigmoid(swish_alpha * gated) * (linear + 1.0)).astype(jnp.bfloat16)
    partial_value = jnp.einsum(
        "sjcf,jfd->sjcd", activated, w_down, preferred_element_type=jnp.float32
    ).astype(jnp.bfloat16)
    summed = sent_and_summed(partial_value, "tp", 3).astype(jnp.bfloat16)
    returned = exchange_by_chip(summed, ("ep_0", "ep_1"), (1, 0), 0, 0)
    returned = returned.reshape(experts_all * capacity, returned.shape[3])
    picked = returned[dest_row].reshape(tok_rows, top_count, returned.shape[1]).astype(jnp.float32)
    return jnp.sum(picked * gate_weights[:, :, None], axis=1).astype(jnp.bfloat16)


def solution(mesh):
    torus = Mesh(
        mesh.devices.reshape(mesh.shape["grp"], 32, 2, mesh.shape["tp"]),
        ("grp", "ep_0", "ep_1", "tp"),
    )
    return jax.shard_map(
        body,
        mesh=torus,
        in_specs=(
            P(GRP_EP, None),
            P(),
            P(EP, None, "tp"),
            P(EP, None, "tp"),
            P(EP, "tp", None),
            P(GRP_EP, None),
            P(GRP_EP, None),
        ),
        out_specs=P(GRP_EP, "tp"),
        check_vma=False,
    )
```

profile of v0, /device:TPU:33, one launch (start us, length us, event | category | flops | bytes accessed | tf_op | source)
XLA Modules:
  0.0 449.6 jit_solution(9208010235505050856)
XLA Ops:
  6.5 0.0 copy-start
  6.6 0.0 all-gather.2.cloned.1.call-start
  6.6 0.9 copy.23
  7.4 0.1 eq.29
  7.6 0.1 eq.25
  7.7 0.7 broadcast_multiply_fusion
  8.4 1.8 reduce-window.6
  10.2 0.3 slice_reduce_fusion
  10.5 0.1 copy.22
  10.6 0.1 mul.68
  10.7 0.1 fusion.26
  10.9 3.4 scatter_custom_fusion
  14.3 1.4 fusion
  15.7 1.4 fusion.2
  17.1 0.1 concatenate.3
  17.2 6.0 %gather_fusion = bf16[1024,2048]{1,0:T(8,128)(2,1)} fusion(bf16[193,2048]{1,0:T(8,128)(2,1)S(1)} %concatenate.3, s32[1024]{0:T(1024)S(1)} %fusion.30), kind=kCustom, calls=%fused_computation | custom fusion | bytes 8392704 | tf_op jit(solution)/shard_map/gather | solution.py:72
  23.2 1.3 constant_dynamic-slice_fusion
  24.5 0.1 copy.26
  24.6 0.0 copy-start.2
  24.6 45.8 %all_to_all.25 = bf16[32,2,1,16,512]{4,3,0,2,1:T(8,128)(2,1)S(1)} all-to-all(bf16[32,2,1,16,512]{4,3,0,2,1:T(8,128)(2,1)S(1)} %copy.26), channel_id=1, replica_groups=mesh['grp'=2,'ep_0'=32,'ep_1'=2,'tp'=4] {'ep_1'}, dimensions={1} | all-to-all | bytes 2097152 | tf_op jit(solution)/shard_map/all_to_all | solution.py:29
  70.4 0.1 copy.27
  70.5 110.0 %all_to_all.26 = bf16[32,2,1,16,512]{4,3,1,2,0:T(8,128)(2,1)} all-to-all(bf16[32,2,1,16,512]{4,3,1,2,0:T(8,128)(2,1)S(1)} %copy.27), channel_id=1, replica_groups=mesh['grp'=2,'ep_0'=32,'ep_1'=2,'tp'=4] {'ep_0'}, dimensions={0} | all-to-all | bytes 2097152 | tf_op jit(solution)/shard_map/all_to_all | solution.py:29
  180.5 0.0 copy-start.3
  180.5 0.1 all-gather.2.cloned.1.call-update
  180.5 51.5 %all-gather.2.cloned.1.call-done = bf16[64,16,2048]{2,1,0:T(8,128)(2,1)} async-done(((bf16[64,16,512]{2,1,0:T(8,128)(2,1)}), bf16[64,16,2048]{2,1,0:T(8,128)(2,1)}) %all-gather.2.cloned.1.call-update) | async-done | bytes 4194320 | tf_op jit(solution)/shard_map/all_gather | solution.py:76
  232.1 0.0 copy-done.2
  232.1 4.5 %fusion.3 = f32[64,1,16,256]{3,2,0,1:T(8,128)} fusion(bf16[64,16,2048]{2,1,0:T(8,128)(2,1)} %all-gather.2.cloned.1.call-done, bf16[1,2048,256]{2,1,0:T(8,128)(2,1)S(1)} %copy-done.2), kind=kOutput, calls=%fused_computation.12 | convolution fusion | flops 1074003968 | bytes 6291456 | tf_op jit(solution)/shard_map/sjcd,jdf->sjcf/dot_general | solution.py:78
  236.6 0.0 copy-done
  236.6 0.0 copy-done.3
  236.6 8.9 %convolution_convert_fusion = bf16[64,16,2048]{2,1,0:T(8,128)(2,1)} fusion(bf16[64,16,2048]{2,1,0:T(8,128)(2,1)} %all-gather.2.cloned.1.call-done, bf16[1,256,2048]{2,1,0:T(8,128)(2,1)S(1)} %copy-done, bf16[1,2048,256]{2,1,0:T(8,128)(2,1)S(1)} %copy-done.3, f32[64,1,16,256]{3,2,0,1:T(8,128)} %fusion.3), kind=kOutput, calls=%fused_computation.4 | convolution fusion | flops 2151940096 | bytes 11534336 | tf_op jit(solution)/shard_map/sjcf,jfd->sjcd/dot_general | solution.py:83
  245.4 2.8 copy.36
  248.3 51.3 %all_to_all.27 = bf16[4,64,1,16,512]{4,3,1,2,0:T(8,128)(2,1)} all-to-all(bf16[4,64,1,16,512]{4,3,1,2,0:T(8,128)(2,1)S(1)} %bitcast.77), channel_id=1, replica_groups=mesh['grp'=2,'ep_0'=32,'ep_1'=2,'tp'=4] {'tp'}, dimensions={0} | all-to-all | bytes 8388608 | tf_op jit(solution)/shard_map/all_to_all | solution.py:41
  299.6 3.3 reduce_sum.44
  302.9 0.0 copy-start.1
  302.9 0.1 copy.29
  303.0 6.1 %all_to_all.28 = bf16[32,2,1,1,16,512]{5,4,0,3,2,1:T(8,128)(2,1)S(1)} all-to-all(bf16[32,2,1,1,16,512]{5,4,0,3,2,1:T(8,128)(2,1)S(1)} %copy.29), channel_id=1, replica_groups=mesh['grp'=2,'ep_0'=32,'ep_1'=2,'tp'=4] {'ep_1'}, dimensions={1} | all-to-all | bytes 2097152 | tf_op jit(solution)/shard_map/all_to_all | solution.py:29
  309.1 1.1 copy.30
  310.2 23.4 %all-to-all-start.4 = ((bf16[32,2,1,1,16,512]{5,4,1,3,2,0:T(8,128)(2,1)}), bf16[32,2,1,1,16,512]{5,4,1,3,2,0:T(8,128)(2,1)S(1)}, u32[]{:S(2)}, u32[]{:S(2)}) async-start(bf16[32,2,1,1,16,512]{5,4,1,3,2,0:T(8,128)(2,1)} %copy.30), calls=%async_computation.4 | async-start | bytes 2097152 | tf_op jit(solution)/shard_map/all_to_all | solution.py:29
  333.6 0.0 copy-done.1
  333.6 0.1 copy.31
  333.7 104.2 %all-to-all-done.4 = bf16[32,2,1,1,16,512]{5,4,1,3,2,0:T(8,128)(2,1)S(1)} async-done(((bf16[32,2,1,1,16,512]{5,4,1,3,2,0:T(8,128)(2,1)}), bf16[32,2,1,1,16,512]{5,4,1,3,2,0:T(8,128)(2,1)S(1)}, u32[]{:S(2)}, u32[]{:S(2)}) %all-to-all-start.4) | async-done | bytes 1048608 | tf_op jit(solution)/shard_map/all_to_all | solution.py:29
  437.9 2.7 gather_fusion.1
  440.6 0.5 reshape.102
  441.1 1.7 multiply_reduce_fusion
  (7 shorter events, 0.1 us)
Async XLA Ops:
  6.5 230.0 %copy-start = (bf16[1,256,2048]{2,1,0:T(8,128)(2,1)S(1)}, bf16[1,256,2048]{2,1,0:T(8,128)(2,1)}, u32[]{:S(2)}) copy-start(bf16[1,256,2048]{2,1,0:T(8,128)(2,1)} %param.11) | copy-start | bytes 3145732
  6.6 225.5 %all-gather.2.cloned.1.call-start = ((), (), s32[]{:S(2)}) async-start(), calls=%async_computation.5 | async-start | bytes 5242880 | tf_op jit(solution)/shard_map/all_gather | solution.py:76
  24.6 207.5 %copy-start.2 = (bf16[1,2048,256]{2,1,0:T(8,128)(2,1)S(1)}, bf16[1,2048,256]{2,1,0:T(8,128)(2,1)}, u32[]{:S(2)}) copy-start(bf16[1,2048,256]{2,1,0:T(8,128)(2,1)} %param.9) | copy-start | bytes 3145732
  180.5 56.1 %copy-start.3 = (bf16[1,2048,256]{2,1,0:T(8,128)(2,1)S(1)}, bf16[1,2048,256]{2,1,0:T(8,128)(2,1)}, u32[]{:S(2)}) copy-start(bf16[1,2048,256]{2,1,0:T(8,128)(2,1)} %param.10) | copy-start | bytes 3145732
  302.9 30.7 %copy-start.1 = (f32[192,4]{0,1:T(4,128)S(1)}, f32[192,4]{0,1:T(4,128)}, u32[]{:S(2)}) copy-start(f32[192,4]{0,1:T(4,128)} %param.13) | copy-start | bytes 9220
  310.2 127.7 %all-to-all-start.4 = ((bf16[32,2,1,1,16,512]{5,4,1,3,2,0:T(8,128)(2,1)}), bf16[32,2,1,1,16,512]{5,4,1,3,2,0:T(8,128)(2,1)S(1)}, u32[]{:S(2)}, u32[]{:S(2)}) async-start(bf16[32,2,1,1,16,512]{5,4,1,3,2,0:T(8,128)(2,1)} %copy.30), calls=%async_computation.4 | async-start | bytes 2097152 | tf_op jit(solution)/shard_map/all_to_all | solution.py:29
Sparse Core Ops, SparseCore 0:
  180.7 51.3 all-gather.1
where the time goes:
time: 450 us
  blocking collectives  213 us (47%)
  waiting for transfers between devices  156 us (35%)
  starting transfers between devices  23.4 us (5%)
  local copies, waits for them, and re-layouts  19.8 us (4%)
  between operations  13.6 us (3%)
  matrix products  13.4 us (3%)
  other arithmetic  10.5 us (2%)
    all_to_all x3, blocking collectives, turned_blocks(): whole = lax.all_to_all(whole, axes[k], k, k, tiled=True)  162 us
    all_to_all x1, waiting for transfers between devices, turned_blocks(): whole = lax.all_to_all(whole, axes[k], k, k, tiled=True)  104 us
    all_gather x1, waiting for transfers between devices, body(): received = lax.all_gather(received, 'tp', axis=2, tiled=True)  51.5 us
    all_to_all x1, blocking collectives, sent_and_summed(): lax.all_to_all(blocks, axis, split_axis=0, concat_axis=0, tiled=True)  51.3 us
    all_to_all x1, starting transfers between devices, turned_blocks(): whole = lax.all_to_all(whole, axes[k], k, k, tiled=True)  23.4 us
  transfers between devices with their start and end apart: 2, of which 2 were waited for; matrix products, arithmetic and copies ran while one was open for 0% of the time, Pallas kernels for 0%

commit v1 on v0

--- a/solution.py
+++ b/solution.py
@@ -9,6 +9,28 @@
 epsilon = 1e-06
 clamp_limit = 7.0
 swish_alpha = 1.702
+
+
+def laid_out_2(parts, dim):
+    shape = list(parts.shape[1:])
+    shape[dim] *= parts.shape[0]
+    return jnp.moveaxis(parts, 0, dim).reshape(shape)
+
+
+def gather_around(x, axis, dim):
+    size = lax.axis_size(axis)
+    pairs = [(i, (i + 1) % size) for i in range(size)]
+    back = [(b, a) for a, b in pairs]
+    lower, upper = ([], [])
+    for step in range(size - 1):
+        if step % 2 == 0:
+            lower.append(lax.ppermute(lower[-1] if lower else x, axis, pairs))
+        else:
+            upper.append(lax.ppermute(upper[-1] if upper else x, axis, back))
+    blocks = jnp.stack([*lower[::-1], x, *upper])
+    shift = lax.axis_index(axis) - len(lower)
+    blocks = blocks[(jnp.arange(size) - shift) % size]
+    return laid_out_2(blocks, dim)
 
 
 def cut_along(value, dim, devices):
@@ -73,7 +95,7 @@
     col_share = model_width // tp_count
     col_part = lax.dynamic_slice_in_dim(send_buffer, lax.axis_index("tp") * col_share, col_share, 2)
     received = exchange_by_chip(col_part, ("ep_0", "ep_1"), (1, 0), 0, 0)
-    received = lax.all_gather(received, "tp", axis=2, tiled=True)
+    received = gather_around(received, "tp", 2)
     expert_rows = received.reshape(ep_count, local_experts, capacity, model_width)
     gate_pre = jnp.einsum("sjcd,jdf->sjcf", expert_rows, w_gate, preferred_element_type=jnp.float32)
     up_pre = jnp.einsum("sjcd,jdf->sjcf", expert_rows, w_up, preferred_element_type=jnp.float32)

time: 450 us -> 435 us (0.967)
  between operations: 13.6 us -> 0.27 us
  local copies, waits for them, and re-layouts: 19.8 us -> 29.6 us
  starting transfers between devices: 23.4 us -> 17.4 us
  waiting for transfers between devices: 156 us -> 150 us
    all_gather x1 -> x0, waiting for transfers between devices: 51.5 us -> none  [body(): received = lax.all_gather(received, 'tp', axis=2, tiled=True)]
    ppermute x0 -> x3, waiting for transfers between devices: none -> 45.3 us  [the longest x2 45.3 us: gather_around(): lower.append(lax.ppermute(lower[-1] if lower else x, axis, pairs))]
    all_to_all x1, starting transfers between devices: 23.4 us -> 8.65 us  [turned_blocks(): whole = lax.all_to_all(whole, axes[k], k, k, tiled=True)]
    ppermute x0 -> x3, starting transfers between devices: none -> 8.71 us  [the longest x2 5.21 us: gather_around(): lower.append(lax.ppermute(lower[-1] if lower else x, axis, pairs))]
    gather x0 -> x1, local copies, waits for them, and re-layouts: none -> 4.97 us  [gather_around(): blocks = blocks[(jnp.arange(size) - shift) % size]]
  transfers between devices with their start and end apart: 2 -> 4, of which waited for: 2 -> 3; matrix products, arithmetic and copies ran while one was open for 0% -> 0% of each run, Pallas kernels for 0% -> 0%
where the time goes in v1:
time: 435 us; the launch traced here: 434 us
  blocking collectives  213 us (49%)
  waiting for transfers between devices  150 us (34%)
  local copies, waits for them, and re-layouts  29.6 us (7%)
  starting transfers between devices  17.4 us (4%)
  other arithmetic  13.9 us (3%)
  matrix products  9.8 us (2%)
    all_to_all x3, blocking collectives, turned_blocks(): whole = lax.all_to_all(whole, axes[k], k, k, tiled=True)  163 us
    all_to_all x1, waiting for transfers between devices, turned_blocks(): whole = lax.all_to_all(whole, axes[k], k, k, tiled=True)  105 us
    all_to_all x1, blocking collectives, sent_and_summed(): lax.all_to_all(blocks, axis, split_axis=0, concat_axis=0, tiled=True)  49.9 us
    ppermute x2, waiting for transfers between devices, gather_around(): lower.append(lax.ppermute(lower[-1] if lower else x, axis, pairs))  45.3 us
  transfers between devices with their start and end apart: 4, of which 3 were waited for; matrix products, arithmetic and copies ran while one was open for 0% of the time, Pallas kernels for 0%

profile of v1, /device:TPU:33, one launch (start us, length us, event | category | flops | bytes accessed | tf_op | source)
XLA Modules:
  0.0 433.9 jit_solution(7259692507942186997)
XLA Ops:
  0.0 0.0 copy-start
  0.0 0.9 copy.30
  0.9 0.1 eq.31
  1.0 0.1 eq.27
  1.1 0.7 broadcast_multiply_fusion
  1.8 1.8 reduce-window.6
  3.6 0.3 slice_reduce_fusion
  3.9 0.1 copy.29
  4.1 0.1 mul.68
  4.2 0.1 fusion.26
  4.3 3.4 scatter_custom_fusion
  7.7 1.4 fusion
  9.1 1.4 fusion.2
  10.5 0.1 concatenate.3
  10.6 6.0 %gather_fusion = bf16[1024,2048]{1,0:T(8,128)(2,1)} fusion(bf16[193,2048]{1,0:T(8,128)(2,1)S(1)} %concatenate.3, s32[1024]{0:T(1024)S(1)} %fusion.30), kind=kCustom, calls=%fused_computation | custom fusion | bytes 8392704 | tf_op jit(solution)/shard_map/gather | solution.py:94
  16.6 1.3 constant_dynamic-slice_fusion
  17.9 0.1 copy.33
  18.0 45.6 %all_to_all.25 = bf16[32,2,1,16,512]{4,3,0,2,1:T(8,128)(2,1)S(1)} all-to-all(bf16[32,2,1,16,512]{4,3,0,2,1:T(8,128)(2,1)S(1)} %copy.33), channel_id=1, replica_groups=mesh['grp'=2,'ep_0'=32,'ep_1'=2,'tp'=4] {'ep_1'}, dimensions={1} | all-to-all | bytes 2097152 | tf_op jit(solution)/shard_map/all_to_all | solution.py:51
  63.7 0.1 copy.34
  63.8 109.9 %all_to_all.26 = bf16[32,2,1,16,512]{4,3,1,2,0:T(8,128)(2,1)S(1)} all-to-all(bf16[32,2,1,16,512]{4,3,1,2,0:T(8,128)(2,1)S(1)} %copy.34), channel_id=1, replica_groups=mesh['grp'=2,'ep_0'=32,'ep_1'=2,'tp'=4] {'ep_0'}, dimensions={0} | all-to-all | bytes 2097152 | tf_op jit(solution)/shard_map/all_to_all | solution.py:51
  173.7 3.3 collective-permute-start
  177.0 3.5 collective-permute-start.2
  180.5 20.8 %collective-permute-done = bf16[64,16,512]{2,1,0:T(8,128)(2,1)S(1)} collective-permute-done((bf16[64,16,512]{2,1,0:T(8,128)(2,1)S(1)}, bf16[64,16,512]{2,1,0:T(8,128)(2,1)S(1)}, u32[]{:S(2)}, u32[]{:S(2)}) %collective-permute-start) | collective-permute-done | bytes 1048608 | tf_op jit(solution)/shard_map/ppermute | solution.py:27
  201.2 1.9 collective-permute-start.1
  203.2 0.0 collective-permute-done.2
  203.2 24.6 %collective-permute-done.1 = bf16[64,16,512]{2,1,0:T(8,128)(2,1)} collective-permute-done((bf16[64,16,512]{2,1,0:T(8,128)(2,1)S(1)}, bf16[64,16,512]{2,1,0:T(8,128)(2,1)}, u32[]{:S(2)}, u32[]{:S(2)}) %collective-permute-start.1) | collective-permute-done | bytes 1048608 | tf_op jit(solution)/shard_map/ppermute | solution.py:27
  227.8 3.4 pad_maximum_fusion
  231.2 5.0 %gather_fusion.1 = bf16[4,64,16,512]{3,2,1,0:T(8,128)(2,1)} fusion(bf16[4,64,16,512]{3,2,1,0:T(8,128)(2,1)} %pad_maximum_fusion, s32[1024]{0:T(1024)S(1)} %pad_clamp_fusion.1), kind=kCustom, calls=%fused_computation.1 | custom fusion | bytes 8388624 | tf_op jit(solution)/shard_map/gather | solution.py:32
  236.2 0.0 copy-start.3
  236.2 2.9 copy.42
  239.1 0.0 copy-start.1
  239.1 0.0 copy-start.4
  239.1 1.9 copy-done.1
  241.0 0.0 copy-done.3
  241.1 1.3 fusion.3
  242.3 0.0 copy-done
  242.3 0.0 copy-done.4
  242.3 8.6 %convolution_convert_fusion = bf16[64,16,2048]{2,1,0:T(8,128)(2,1)} fusion(bf16[64,16,2048]{2,1,0:T(8,128)(2,1)} %bitcast.91, bf16[1,256,2048]{2,1,0:T(8,128)(2,1)S(1)} %copy-done, bf16[1,2048,256]{2,1,0:T(8,128)(2,1)S(1)} %copy-done.4, f32[64,1,16,256]{3,2,0,1:T(8,128)S(1)} %fusion.3), kind=kOutput, calls=%fused_computation.6 | convolution fusion | flops 2151940096 | bytes 11534336 | tf_op jit(solution)/shard_map/sjcf,jfd->sjcd/dot_general | solution.py:105
  250.9 2.8 copy.45
  253.7 49.9 %all_to_all.27 = bf16[4,64,1,16,512]{4,3,1,2,0:T(8,128)(2,1)} all-to-all(bf16[4,64,1,16,512]{4,3,1,2,0:T(8,128)(2,1)S(1)} %bitcast.87), channel_id=1, replica_groups=mesh['grp'=2,'ep_0'=32,'ep_1'=2,'tp'=4] {'tp'}, dimensions={0} | all-to-all | bytes 8388608 | tf_op jit(solution)/shard_map/all_to_all | solution.py:63
  303.6 3.3 reduce_sum.44
  306.9 0.0 copy-start.2
  307.0 0.1 copy.37
  307.0 7.5 %all_to_all.28 = bf16[32,2,1,1,16,512]{5,4,0,3,2,1:T(8,128)(2,1)S(1)} all-to-all(bf16[32,2,1,1,16,512]{5,4,0,3,2,1:T(8,128)(2,1)S(1)} %copy.37), channel_id=1, replica_groups=mesh['grp'=2,'ep_0'=32,'ep_1'=2,'tp'=4] {'ep_1'}, dimensions={1} | all-to-all | bytes 2097152 | tf_op jit(solution)/shard_map/all_to_all | solution.py:51
  314.6 1.1 copy.38
  315.7 8.7 %all-to-all-start.4 = ((bf16[32,2,1,1,16,512]{5,4,1,3,2,0:T(8,128)(2,1)}), bf16[32,2,1,1,16,512]{5,4,1,3,2,0:T(8,128)(2,1)S(1)}, u32[]{:S(2)}, u32[]{:S(2)}) async-start(bf16[32,2,1,1,16,512]{5,4,1,3,2,0:T(8,128)(2,1)} %copy.38), calls=%async_computation.4 | async-start | bytes 2097152 | tf_op jit(solution)/shard_map/all_to_all | solution.py:51
  324.3 0.0 copy-done.2
  324.3 0.1 copy.39
  324.5 104.5 %all-to-all-done.4 = bf16[32,2,1,1,16,512]{5,4,1,3,2,0:T(8,128)(2,1)S(1)} async-done(((bf16[32,2,1,1,16,512]{5,4,1,3,2,0:T(8,128)(2,1)}), bf16[32,2,1,1,16,512]{5,4,1,3,2,0:T(8,128)(2,1)S(1)}, u32[]{:S(2)}, u32[]{:S(2)}) %all-to-all-start.4) | async-done | bytes 1048608 | tf_op jit(solution)/shard_map/all_to_all | solution.py:51
  429.0 2.7 gather_fusion.2
  431.7 0.5 reshape.153
  432.2 1.7 multiply_reduce_fusion
  (9 shorter events, 0.1 us)
Async XLA Ops:
  0.0 242.3 %copy-start = (bf16[1,256,2048]{2,1,0:T(8,128)(2,1)S(1)}, bf16[1,256,2048]{2,1,0:T(8,128)(2,1)}, u32[]{:S(2)}) copy-start(bf16[1,256,2048]{2,1,0:T(8,128)(2,1)} %param.11) | copy-start | bytes 3145732
  173.7 27.5 %collective-permute-start = (bf16[64,16,512]{2,1,0:T(8,128)(2,1)S(1)}, bf16[64,16,512]{2,1,0:T(8,128)(2,1)S(1)}, u32[]{:S(2)}, u32[]{:S(2)}) collective-permute-start(bf16[64,16,512]{2,1,0:T(8,128)(2,1)S(1)} %bitcast.94), channel_id=1, source_target_pairs={{0,1},{1,2},{2,3},{3,0},{4,5},{5,6},{6,7},{7,4},{8,9},{9,10},{10,1... | collective-permute-start | bytes 3145736 | tf_op jit(solution)/shard_map/ppermute | solution.py:27
  177.0 26.2 %collective-permute-start.2 = (bf16[64,16,512]{2,1,0:T(8,128)(2,1)S(1)}, bf16[64,16,512]{2,1,0:T(8,128)(2,1)}, u32[]{:S(2)}, u32[]{:S(2)}) collective-permute-start(bf16[64,16,512]{2,1,0:T(8,128)(2,1)S(1)} %bitcast.95), channel_id=1, source_target_pairs={{1,0},{2,1},{3,2},{0,3},{5,4},{6,5},{7,6},{4,7},{9,8},{10,9},{11,1... | collective-permute-start | bytes 3145736 | tf_op jit(solution)/shard_map/ppermute | solution.py:29
  201.2 26.6 %collective-permute-start.1 = (bf16[64,16,512]{2,1,0:T(8,128)(2,1)S(1)}, bf16[64,16,512]{2,1,0:T(8,128)(2,1)}, u32[]{:S(2)}, u32[]{:S(2)}) collective-permute-start(bf16[64,16,512]{2,1,0:T(8,128)(2,1)S(1)} %collective-permute-done), channel_id=1, source_target_pairs={{0,1},{1,2},{2,3},{3,0},{4,5},{5,6},{6,7},{7,4},{8,9},{9,10},{10,1... | collective-permute-start | bytes 3145736 | tf_op jit(solution)/shard_map/ppermute | solution.py:27
  236.2 4.9 %copy-start.3 = (bf16[1,2048,256]{2,1,0:T(8,128)(2,1)S(1)}, bf16[1,2048,256]{2,1,0:T(8,128)(2,1)}, u32[]{:S(2)}) copy-start(bf16[1,2048,256]{2,1,0:T(8,128)(2,1)} %param.9) | copy-start | bytes 3145732
  239.1 1.9 copy-start.1
  239.1 3.2 copy-start.4
  306.9 17.4 %copy-start.2 = (f32[192,4]{0,1:T(4,128)S(1)}, f32[192,4]{0,1:T(4,128)}, u32[]{:S(2)}) copy-start(f32[192,4]{0,1:T(4,128)} %param.13) | copy-start | bytes 9220
  315.7 113.3 %all-to-all-start.4 = ((bf16[32,2,1,1,16,512]{5,4,1,3,2,0:T(8,128)(2,1)}), bf16[32,2,1,1,16,512]{5,4,1,3,2,0:T(8,128)(2,1)S(1)}, u32[]{:S(2)}, u32[]{:S(2)}) async-start(bf16[32,2,1,1,16,512]{5,4,1,3,2,0:T(8,128)(2,1)} %copy.38), calls=%async_computation.4 | async-start | bytes 2097152 | tf_op jit(solution)/shard_map/all_to_all | solution.py:51
